TPU v7x, 32 devices: a whole 2x2x4 slice. The times are simulated.
32 devices in a mesh: kv: 8 (over z, y), tp: 4 (over x, core).
Axes of the slice: x: 2, y: 2, z: 4, core: 2. Of those that a mesh axis runs over, the one named last changes fastest.
Arguments:
- tokens: bfloat16 [16, 4, 4096], P(None, None, 'kv'), may hold values from -20 to 20
- mix_gain: float32 [4096], P('kv'), may hold values from 0.1 to 1.9
- w_query: bfloat16 [4096, 2048], P('kv', 'tp'), may hold values from -0.09375 to 0.09375
- w_key: bfloat16 [4096, 2048], P('kv', 'tp'), may hold values from -0.09375 to 0.09375
- w_value: bfloat16 [4096, 2048], P('kv', 'tp'), may hold values from -0.09375 to 0.09375
- w_forget: bfloat16 [4096, 16], replicated, may hold values from -0.09375 to 0.09375
- forget_bias: float32 [16], P('tp'), may hold values from -1 to 3
- key_cache: bfloat16 [16, 4096, 2048], P(None, 'kv', 'tp'), may hold values from -6 to 6
- value_cache: bfloat16 [16, 4096, 2048], P(None, 'kv', 'tp'), may hold values from -6 to 6
- cum_gate: float32 [16, 16, 4096], P(None, 'tp', 'kv'), may hold values from -761.52 to 0, as said below
- lengths: int32 [16], replicated, may hold values from 1 to 4096, 16381 in all
- w_out: bfloat16 [2048, 4096], P('tp', 'kv'), may hold values from -0.125 to 0.125
- mlp_gain: float32 [4096], P('kv'), may hold values from 0.1 to 1.9
- w_gate: bfloat16 [4096, 11264], P('kv', 'tp'), may hold values from -0.09375 to 0.09375
- w_up: bfloat16 [4096, 11264], P('kv', 'tp'), may hold values from -0.09375 to 0.09375
- w_down: bfloat16 [11264, 4096], P('tp', 'kv'), may hold values from -0.0546875 to 0.0546875
Outputs:
- result: bfloat16 [16, 4, 4096], P(None, None, 'kv')
Inputs may be any that keep to these rules, and one draw needn't show every extreme that they name: `cum_gate`: never rising along positions. `lengths`: one sequence fills all 4096 positions.
All inputs are finite; a program needn't handle non-finite values.
Results may differ from a plain program's by a relative error of at most 0.02.
Values may be sent and summed in bfloat16 or wider, within the bound.
A program may use at most 64 MiB of HBM per device.

v0:
```python
import jax
import jax.numpy as jnp
from jax import lax
from jax.sharding import PartitionSpec as P

D = 4096
EPSILON = 1e-06
NEG_FILL = -1e30


def combined_all(array, axis, combine):
    everything = jax.tree.map(lambda part: lax.all_gather(part, axis), array)
    first = jax.tree.map(lambda part: part[0], everything)

    def turn(k, so_far):
        return combine(so_far, jax.tree.map(lambda part: part[k], everything))

    return lax.fori_loop(1, lax.axis_size(axis), turn, first)


def on_device(
    tokens,
    mix_gain,
    w_query,
    w_key,
    w_value,
    w_forget,
    forget_bias,
    key_cache,
    value_cache,
    cum_gate,
    lengths,
    w_out,
    mlp_gain,
    w_gate,
    w_up,
    w_down,
):
    seq_count, new_count, local_width = tokens.shape
    row_count = seq_count * new_count
    heads_dev = forget_bias.shape[0]
    head_width = w_query.shape[1] // heads_dev
    pos_dev = key_cache.shape[1]
    kv_index = lax.axis_index("kv")
    tp_index = lax.axis_index("tp")
    inputs = tokens.reshape(row_count, local_width).astype(jnp.float32)
    scaled = (inputs * mix_gain).astype(jnp.bfloat16)
    forget_rows = lax.dynamic_slice_in_dim(w_forget, kv_index * local_width, local_width, 0)
    forget_cols = lax.dynamic_slice_in_dim(forget_rows, tp_index * heads_dev, heads_dev, 1)
    query_part = jnp.dot(scaled, w_query, preferred_element_type=jnp.float32)
    key_part = jnp.dot(scaled, w_key, preferred_element_type=jnp.float32)
    value_part = jnp.dot(scaled, w_value, preferred_element_type=jnp.float32)
    forget_part = jnp.dot(scaled, forget_cols, preferred_element_type=jnp.float32)
    squares = jnp.sum(inputs * inputs, axis=1)
    query_sum, key_sum, value_sum, forget_sum, square_sum = (
        lax.psum(query_part.astype(jnp.bfloat16), "kv").astype(jnp.float32),
        lax.psum(key_part.astype(jnp.bfloat16), "kv").astype(jnp.float32),
        lax.psum(value_part.astype(jnp.bfloat16), "kv").astype(jnp.float32),
        lax.psum(forget_part.astype(jnp.bfloat16), "kv").astype(jnp.float32),
        lax.psum(squares.astype(jnp.bfloat16), "kv").astype(jnp.float32),
    )
    inv_norm = lax.rsqrt(square_sum / D + EPSILON)[:, None]
    head_shape = (seq_count, new_count, heads_dev, head_width)
    query = (inv_norm * query_sum).astype(jnp.bfloat16).reshape(head_shape)
    key_new = (inv_norm * key_sum).astype(jnp.bfloat16).reshape(head_shape)
    value_new = (inv_norm * value_sum).astype(jnp.bfloat16).reshape(head_shape)
    log_forget = jax.nn.log_sigmoid(inv_norm * forget_sum + forget_bias).reshape(
        seq_count, new_count, heads_dev
    )
    score_scale = head_width ** (-0.5)
    positions = kv_index * pos_dev + jnp.arange(pos_dev, dtype=jnp.int32)
    live_rows = positions[None, :] < lengths[:, None]
    live_mask = live_rows[:, None, None, :]
    cached_keys = key_cache.reshape(seq_count, pos_dev, heads_dev, head_width)
    cached_values = value_cache.reshape(seq_count, pos_dev, heads_dev, head_width)
    scores = jnp.einsum("bthd,bphd->bthp", query, cached_keys, preferred_element_type=jnp.float32)
    scores = scores * score_scale - cum_gate[:, None]
    scores = jnp.where(live_mask, scores, NEG_FILL)
    block_peak = jnp.max(scores, axis=3)
    weights = jnp.where(live_mask, jnp.exp(scores - block_peak[..., None]), 0.0)
    block_total = jnp.sum(weights, axis=3)
    block_sum = jnp.einsum(
        "bthp,bphd->bthd",
        weights.astype(jnp.bfloat16),
        cached_values,
        preferred_element_type=jnp.float32,
    )
    last_hit = positions[None, :] == (lengths - 1)[:, None]
    last_piece = jnp.sum(jnp.where(last_hit[:, None, :], cum_gate, 0.0), axis=2)

    def combine(first, second):
        peak_both = jnp.maximum(first[0], second[0])
        first_factor = jnp.exp(first[0] - peak_both)
        second_factor = jnp.exp(second[0] - peak_both)
        return (
            peak_both,
            first[1] * first_factor + second[1] * second_factor,
            first[2] * first_factor[..., None] + second[2] * second_factor[..., None],
            first[3] + second[3],
        )

    past_peak, past_total, past_sum, last_cum = combined_all(
        (block_peak, block_total, block_sum, last_piece), "kv", combine
    )
    key_cum = last_cum[:, None, :] + jnp.cumsum(log_forget, axis=1)
    own_scores = (
        jnp.einsum("bthd,bshd->bths", query, key_new, preferred_element_type=jnp.float32)
        * score_scale
    )
    own_scores = own_scores - jnp.transpose(key_cum, (0, 2, 1))[:, None]
    causal = (jnp.arange(new_count)[:, None] >= jnp.arange(new_count)[None, :])[None, :, None, :]
    own_scores = jnp.where(causal, own_scores, NEG_FILL)
    peak_score = jnp.maximum(past_peak, jnp.max(own_scores, axis=3))
    past_factor = jnp.exp(past_peak - peak_score)
    own_weights = jnp.where(causal, jnp.exp(own_scores - peak_score[..., None]), 0.0)
    numerator = past_sum * past_factor[..., None] + jnp.einsum(
        "bths,bshd->bthd",
        own_weights.astype(jnp.bfloat16),
        value_new,
        preferred_element_type=jnp.float32,
    )
    denominator = past_total * past_factor + jnp.sum(own_weights, axis=3)
    attended = (
        (numerator / denominator[..., None])
        .astype(jnp.bfloat16)
        .reshape(row_count, heads_dev * head_width)
    )
    attn_out = lax.psum(
        jnp.dot(attended, w_out, preferred_element_type=jnp.float32).astype(jnp.bfloat16), "tp"
    ).astype(jnp.float32)
    middle = (inputs + attn_out).astype(jnp.bfloat16)
    middle_wide = middle.astype(jnp.float32)
    squares2 = jnp.sum(middle_wide * middle_wide, axis=1)
    scaled2 = (middle_wide * mlp_gain).astype(jnp.bfloat16)
    gate_part = jnp.dot(scaled2, w_gate, preferred_element_type=jnp.float32)
    up_part = jnp.dot(scaled2, w_up, preferred_element_type=jnp.float32)
    gate_sum, up_sum, square_sum2 = (
        lax.psum(gate_part.astype(jnp.bfloat16), "kv").astype(jnp.float32),
        lax.psum(up_part.astype(jnp.bfloat16), "kv").astype(jnp.float32),
        lax.psum(squares2.astype(jnp.bfloat16), "kv").astype(jnp.float32),
    )
    inv_norm2 = lax.rsqrt(square_sum2 / D + EPSILON)[:, None]
    hidden = (jax.nn.silu(inv_norm2 * gate_sum) * (inv_norm2 * up_sum)).astype(jnp.bfloat16)
    down_part = jnp.dot(hidden, w_down, preferred_element_type=jnp.float32)
    mixed = lax.psum(down_part.astype(jnp.bfloat16), "tp").astype(jnp.float32)
    return (middle_wide + mixed).astype(jnp.bfloat16).reshape(seq_count, new_count, local_width)


def solution(mesh):
    in_specs = (
        P(None, None, "kv"),
        P("kv"),
        P("kv", "tp"),
        P("kv", "tp"),
        P("kv", "tp"),
        P(),
        P("tp"),
        P(None, "kv", "tp"),
        P(None, "kv", "tp"),
        P(None, "tp", "kv"),
        P(),
        P("tp", "kv"),
        P("kv"),
        P("kv", "tp"),
        P("kv", "tp"),
        P("tp", "kv"),
    )
    out_specs = P(None, None, "kv")
    return jax.shard_map(
        on_device, mesh=mesh, in_specs=in_specs, out_specs=out_specs, check_vma=False
    )
```

profile of v0, /device:TPU:0, one launch (start us, length us, event | category | flops | bytes accessed | tf_op | source)
XLA Modules:
  0.0 381.2 jit_solution(16673894785011786111)
XLA Ops:
  6.5 1.0 reshape.113
  8.2 1.9 convolution_convert_fusion.4
  10.1 1.9 convolution_convert_fusion.5
  12.0 1.9 convolution_convert_fusion.6
  13.9 1.0 multiply_reduce_fusion
  15.7 1.3 broadcast_compare_fusion
  17.0 0.9 convolution_convert_fusion.7
  17.9 23.7 %all-reduce = (bf16[64]{0:T(256)(128)(2,1)S(1)}, bf16[64,4]{0,1:T(4,128)(2,1)}) all-reduce(bf16[64]{0:T(256)(128)(2,1)S(1)} %convert_element_type.112, bf16[64,4]{0,1:T(4,128)(2,1)S(1)} %convolution_convert_fusion.7), channel_id=1, replica_groups=mesh['kv'=8,'tp'=4] {'kv'}, use_global_device_ids=true, to_apply=%region_1.0 | all-reduce | flops 320 | bytes 1280 | tf_op jit(solution)/shard_map/psum | solution.py:60
  41.7 46.5 %all-reduce.14.cloned.1.call-done = (bf16[64,512]{1,0:T(8,128)(2,1)}, bf16[64,512]{1,0:T(8,128)(2,1)}, bf16[64,512]{1,0:T(8,128)(2,1)}) async-done(((bf16[64,512]{1,0:T(8,128)(2,1)}, bf16[64,512]{1,0:T(8,128)(2,1)}, bf16[64,512]{1,0:T(8,128)(2,1)}), (bf16[64,512]{1,0:T(8,128)(2,1)}, bf16[64,512]{1,0:T(8,128)(2,1)}, bf16[64,512]{1,0:T(8,128)(2,1)})) %all-reduce.14.cloned.1.call-update) | async-done | bytes 196624 | tf_op jit(solution)/shard_map/psum | solution.py:56
  88.1 1.6 multiply_convert_fusion.2
  90.4 5.9 %fusion.55 = (f32[16,4,4]{1,2,0:T(4,128)S(1)}, f32[16,4,4,512]{3,1,2,0:T(4,128)S(1)}) fusion(f32[16,4,512]{2,1,0:T(4,128)} %param.27, bf16[16,4,4,128]{3,2,1,0:T(4,128)(2,1)} %reshape.105, pred[16,512]{1,0:T(8,128)(4,1)S(1)} %get-tuple-element.304, bf16[16,512,512]{2,1,0:T(8,128)(2,1)} %param.25), kind=kOutput, calls=%fused_computation.83 | convolution fusion | flops 34078464 | bytes 9118720 | tf_op jit(solution)/shard_map/bthd,bphd->bthp/dot_general | solution.py:76
  96.9 1.3 fusion.15
  99.0 1.6 select_reduce_fusion
  101.4 0.8 fusion.50
  102.9 2.9 reduce_window_sum.11
  105.7 26.1 %all-gather.4 = f32[8,16,4]{1,2,0:T(4,128)S(1)} all-gather(f32[1,16,4]{1,2,0:T(4,128)S(1)} %bitcast.110), channel_id=5, replica_groups=mesh['kv'=8,'tp'=4] {'kv'}, dimensions={0}, use_global_device_ids=true | all-gather | bytes 2304 | tf_op jit(solution)/shard_map/all_gather | solution.py:12
  132.5 1.5 copy.88
  134.0 1.5 reshape.110
  135.5 1.5 reshape.108
  137.0 1.7 fusion.41
  138.7 1.7 copy.101
  140.4 1.8 fusion.27
  142.2 1.0 copy.89
  143.1 30.9 %all-gather.1 = f32[128,4,4]{2,1,0:T(4,128)S(1)} all-gather(f32[16,4,4]{2,1,0:T(4,128)S(1)} %copy.89), channel_id=3, replica_groups=mesh['kv'=8,'tp'=4] {'kv'}, dimensions={0}, use_global_device_ids=true | all-gather | bytes 9216 | tf_op jit(solution)/shard_map/all_gather | solution.py:12
  174.4 31.0 %all-gather = f32[128,4,4]{2,1,0:T(4,128)S(1)} all-gather(f32[16,4,4]{2,1,0:T(4,128)} %copy.88), channel_id=2, replica_groups=mesh['kv'=8,'tp'=4] {'kv'}, dimensions={0}, use_global_device_ids=true | all-gather | bytes 9216 | tf_op jit(solution)/shard_map/all_gather | solution.py:12
  205.7 0.9 slice.23
  206.7 15.8 %while.21 = (s32[]{:T(128)}, f32[16,4,4]{0,2,1:T(4,128)S(1)}, f32[16,4,4]{0,2,1:T(4,128)S(1)}, f32[16,4,4,128]{3,2,1,0:T(4,128)S(1)}, f32[16,4]{0,1:T(4,128)S(1)...) while((s32[]{:T(128)}, f32[16,4,4]{0,2,1:T(4,128)S(1)}, ...), condition=%wide.region_7.8_spmd, body=%wide.region_6.7_spmd.sunk | while | flops 99909 | bytes 408483 | solution.py:18
  207.6 1.3 fusion.73
  209.9 1.3 fusion.73
  212.1 1.3 fusion.73
  214.4 1.3 fusion.73
  216.7 1.3 fusion.73
  218.9 1.3 fusion.73
  221.2 1.3 fusion.73
  222.5 0.8 add_bitcast_fusion
  223.4 0.9 fusion.51
  224.3 0.9 fusion.47
  225.4 1.0 fusion.39
  226.6 1.9 convolution_convert_fusion.3
  228.6 29.2 %all-reduce.8.cloned.1.call-done = bf16[64,512]{1,0:T(8,128)(2,1)} async-done(((bf16[64,512]{1,0:T(8,128)(2,1)}), bf16[64,512]{1,0:T(8,128)(2,1)}) %all-reduce.8.cloned.1.call-update) | async-done | bytes 65552 | tf_op jit(solution)/shard_map/psum | solution.py:128
  257.8 1.0 fusion.32
  258.8 2.0 convolution_convert_fusion.1
  260.8 3.2 convolution_convert_fusion
  264.1 21.6 %psum.76 = bf16[64]{0:T(256)(128)(2,1)S(1)} all-reduce(bf16[64]{0:T(256)(128)(2,1)S(1)} %get-tuple-element.297), channel_id=1, replica_groups=mesh['kv'=8,'tp'=4] {'kv'}, use_global_device_ids=true, to_apply=%region_16.17 | all-reduce | flops 64 | bytes 256 | tf_op jit(solution)/shard_map/psum | solution.py:140
  285.7 53.3 %all-reduce.12.cloned.1.call-done = (bf16[64,2816]{1,0:T(8,128)(2,1)}, bf16[64,2816]{1,0:T(8,128)(2,1)}) async-done(((bf16[64,2816]{1,0:T(8,128)(2,1)}, bf16[64,2816]{1,0:T(8,128)(2,1)}), (bf16[64,2816]{1,0:T(8,128)(2,1)}, bf16[64,2816]{1,0:T(8,128)(2,1)})) %all-reduce.12.cloned.1.call-update) | async-done | bytes 720912 | tf_op jit(solution)/shard_map/psum | solution.py:139
  338.9 3.4 convolution_convert_fusion.2
  342.3 30.8 %all-reduce.10.cloned.1.call-done = bf16[64,512]{1,0:T(8,128)(2,1)} async-done(((bf16[64,512]{1,0:T(8,128)(2,1)}), bf16[64,512]{1,0:T(8,128)(2,1)}) %all-reduce.10.cloned.1.call-update) | async-done | bytes 65552 | tf_op jit(solution)/shard_map/psum | solution.py:145
  373.1 0.9 fusion.34
  (74 shorter events, 14.1 us)
Async XLA Ops:
  6.5 252.3 %copy-start = (bf16[512,2816]{1,0:T(8,128)(2,1)S(1)}, bf16[512,2816]{1,0:T(8,128)(2,1)}, u32[]{:S(2)}) copy-start(bf16[512,2816]{1,0:T(8,128)(2,1)} %param.31) | copy-start | bytes 8650756
  6.5 81.6 %all-reduce.14.cloned.1.call-start = ((), (), s32[]{:S(2)}) async-start(), calls=%async_computation.4 | async-start | bytes 393216 | tf_op jit(solution)/shard_map/psum | solution.py:56
  13.9 191.8 %all-gather.7.cloned.1.call-start = ((), (), s32[]{:S(2)}) async-start(), calls=%async_computation.2 | async-start | bytes 1179648 | tf_op jit(solution)/shard_map/all_gather | solution.py:12
  41.7 48.8 %copy-start.3 = (f32[64]{0:T(128)}, f32[64]{0:T(128)S(1)}, u32[]{:S(2)}) copy-start(f32[64]{0:T(128)S(1)} %add_rsqrt_fusion.1) | copy-start | bytes 772
  90.4 6.5 %copy-start.4 = (bf16[16,512,512]{2,1,0:T(8,128)(2,1)S(1)}, bf16[16,512,512]{2,1,0:T(8,128)(2,1)}, u32[]{:S(2)}) copy-start(bf16[16,512,512]{2,1,0:T(8,128)(2,1)} %param.26) | copy-start | bytes 25165828
  96.3 0.6 copy-start.1
  98.9 158.9 %all-reduce.8.cloned.1.call-start = ((), (), s32[]{:S(2)}) async-start(), calls=%async_computation | async-start | bytes 131072 | tf_op jit(solution)/shard_map/psum | solution.py:128
  131.9 0.6 copy-start.2
  228.5 110.4 %all-reduce.12.cloned.1.call-start = ((), (), s32[]{:S(2)}) async-start(), calls=%async_computation.3 | async-start | bytes 1441792 | tf_op jit(solution)/shard_map/psum | solution.py:139
  264.0 109.1 %all-reduce.10.cloned.1.call-start = ((), (), s32[]{:S(2)}) async-start(), calls=%async_computation.1 | async-start | bytes 131072 | tf_op jit(solution)/shard_map/psum | solution.py:145
Sparse Core Ops, SparseCore 0:
  14.0 74.0 all-reduce.13
  99.0 39.8 all-gather.6
  228.7 29.1 all-reduce.7
  264.2 74.7 all-reduce.11
  342.4 30.6 all-reduce.9
where the time goes:
time: 383 us; the launch traced here: 381 us
  waiting for transfers between devices  160 us (42%)
  blocking collectives  133 us (35%)
  other arithmetic  31.2 us (8%)
  matrix products  26.9 us (7%)
  local copies, waits for them, and re-layouts  16.3 us (4%)
  between operations  13.3 us (3%)
    all_gather x3, blocking collectives, combined_all(): everything = jax.tree.map(lambda part: lax.all_gather(part, axis), array)  88 us
    psum x1, waiting for transfers between devices, on_device(): lax.psum(up_part.astype(jnp.bfloat16), 'kv').astype(jnp.float32)  53.3 us
    psum x1, waiting for transfers between devices, on_device(): lax.psum(query_part.astype(jnp.bfloat16), 'kv').astype(jnp.float32)  46.5 us
    psum x1, waiting for transfers between devices, on_device(): mixed = lax.psum(down_part.astype(jnp.bfloat16), 'tp').astype(jnp.float32)  30.8 us
    psum x1, waiting for transfers between devices, on_device(): lax.psum(jnp.dot(attended, w_out, preferred_element_type=jnp.float32).ast...  29.2 us
    psum x1, blocking collectives, on_device(): lax.psum(squares.astype(jnp.bfloat16), 'kv').astype(jnp.float32)  23.7 us
    psum x1, blocking collectives, on_device(): lax.psum(squares2.astype(jnp.bfloat16), 'kv').astype(jnp.float32)  21.6 us
    add x7, other arithmetic, combine(): first[2] * first_factor[..., None] + second[2] * second_factor[..., None]  9.27 us
  transfers between devices with their start and end apart: 5, of which 4 were waited for; matrix products, arithmetic and copies ran while one was open for 6% of the time, Pallas kernels for 0%

commit v1 on v0

--- a/solution.py
+++ b/solution.py
@@ -53,7 +53,7 @@
     forget_part = jnp.dot(scaled, forget_cols, preferred_element_type=jnp.float32)
     squares = jnp.sum(inputs * inputs, axis=1)
     query_sum, key_sum, value_sum, forget_sum, square_sum = (
-        lax.psum(query_part.astype(jnp.bfloat16), "kv").astype(jnp.float32),
+        jnp.sum(lax.all_gather(query_part.astype(jnp.bfloat16), "kv"), axis=0).astype(jnp.float32),
         lax.psum(key_part.astype(jnp.bfloat16), "kv").astype(jnp.float32),
         lax.psum(value_part.astype(jnp.bfloat16), "kv").astype(jnp.float32),
         lax.psum(forget_part.astype(jnp.bfloat16), "kv").astype(jnp.float32),

time: 383 us -> 354 us (0.924)
  waiting for transfers between devices: 160 us -> 113 us
  blocking collectives: 133 us -> 165 us
  other arithmetic: 31.2 us -> 24.1 us
  local copies, waits for them, and re-layouts: 16.3 us -> 12.1 us
    psum x1, waiting for transfers between devices: 46.5 us -> 0.02 us  [on_device(): lax.psum(key_part.astype(jnp.bfloat16), 'kv').astype(jnp.float32)]
    all_gather x0 -> x1, blocking collectives: none -> 31.5 us  [on_device(): lax.all_gather(query_part.astype(jnp.bfloat16), 'kv')]
    add x7, other arithmetic: 4.77 us -> 0.1 us  [combine(): first[3] + second[3]]
  transfers between devices with their start and end apart: 5 -> 5, of which waited for: 4 -> 3; matrix products, arithmetic and copies ran while one was open for 6% -> 8% of each run, Pallas kernels for 0% -> 0%
where the time goes in v1:
time: 354 us; the launch traced here: 352 us
  blocking collectives  165 us (47%)
  waiting for transfers between devices  113 us (32%)
  matrix products  24.4 us (7%)
  other arithmetic  24.1 us (7%)
  between operations  13.3 us (4%)
  local copies, waits for them, and re-layouts  12.1 us (3%)
    all_gather x3, blocking collectives, combined_all(): everything = jax.tree.map(lambda part: lax.all_gather(part, axis), array)  88.3 us
    psum x1, waiting for transfers between devices, on_device(): lax.psum(up_part.astype(jnp.bfloat16), 'kv').astype(jnp.float32)  53.1 us
    all_gather x1, blocking collectives, on_device(): lax.all_gather(query_part.astype(jnp.bfloat16), 'kv')  31.5 us
    psum x1, waiting for transfers between devices, on_device(): mixed = lax.psum(down_part.astype(jnp.bfloat16), 'tp').astype(jnp.float32)  30.8 us
    psum x1, waiting for transfers between devices, on_device(): lax.psum(jnp.dot(attended, w_out, preferred_element_type=jnp.float32).ast...  28.8 us
    psum x1, blocking collectives, on_device(): lax.psum(squares.astype(jnp.bfloat16), 'kv').astype(jnp.float32)  23.8 us
    psum x1, blocking collectives, on_device(): lax.psum(squares2.astype(jnp.bfloat16), 'kv').astype(jnp.float32)  21.6 us
    add x7, other arithmetic, combine(): first[2] * first_factor[..., None] + second[2] * second_factor[..., None]  9.26 us
  transfers between devices with their start and end apart: 5, of which 3 were waited for; matrix products, arithmetic and copies ran while one was open for 8% of the time, Pallas kernels for 0%

profile of v1, /device:TPU:0, one launch (start us, length us, event | category | flops | bytes accessed | tf_op | source)
XLA Modules:
  0.0 352.3 jit_solution(3205862578022344178)
XLA Ops:
  6.5 1.0 reshape.118
  7.5 0.7 multiply_convert_fusion.5
  8.2 1.9 convolution_convert_fusion.4
  10.1 1.9 convolution_convert_fusion.5
  12.1 1.0 multiply_reduce_fusion
  13.6 1.2 broadcast_add_fusion
  14.9 0.9 convolution_convert_fusion.7
  15.8 23.8 %all-reduce = (bf16[64]{0:T(256)(128)(2,1)S(1)}, bf16[64,4]{0,1:T(4,128)(2,1)}) all-reduce(bf16[64]{0:T(256)(128)(2,1)S(1)} %convert_element_type.119, bf16[64,4]{0,1:T(4,128)(2,1)S(1)} %convolution_convert_fusion.7), channel_id=1, replica_groups=mesh['kv'=8,'tp'=4] {'kv'}, use_global_device_ids=true, to_apply=%region_1.0 | all-reduce | flops 320 | bytes 1280 | tf_op jit(solution)/shard_map/psum | solution.py:60
  40.2 1.2 convolution_convert_fusion.6
  41.5 31.5 %all-gather = bf16[512,512]{1,0:T(8,128)(2,1)S(1)} all-gather(bf16[64,512]{1,0:T(8,128)(2,1)S(1)} %convolution_convert_fusion.6), channel_id=2, replica_groups=mesh['kv'=8,'tp'=4] {'kv'}, dimensions={0}, use_global_device_ids=true | all-gather | bytes 589824 | tf_op jit(solution)/shard_map/all_gather | solution.py:56
  73.0 0.7 reduce_sum.58
  73.7 0.9 reshape.119
  74.6 1.5 broadcast_compare_fusion
  76.3 6.2 %fusion.55 = (f32[16,4,4]{1,2,0:T(4,128)S(1)}, f32[16,4,4,512]{3,1,2,0:T(4,128)S(1)}) fusion(f32[16,4,512]{2,1,0:T(4,128)} %param.27, bf16[16,4,4,128]{3,2,1,0:T(4,128)(2,1)S(1)} %multiply_convert_fusion.4, pred[16,512]{1,0:T(8,128)(4,1)S(1)} %get-tuple-element.303, bf16[16,512,512]{2,1,0:T(8,128)(2,1)} %param.25), kind=kOutput, calls=%fused_computation.83 | convolution fusion | flops 34078464 | bytes 9118720 | tf_op jit(solution)/shard_map/bthd,bphd->bthp/dot_general | solution.py:76
  83.1 1.3 fusion.15
  84.4 0.7 copy.89
  85.1 1.6 copy.86
  86.7 1.0 select_reduce_fusion
  88.4 0.8 fusion.50
  89.2 0.7 reshape.114
  89.9 1.8 fusion.27
  91.6 1.0 copy.87
  92.6 31.1 %all-gather.2 = f32[128,4,4]{2,1,0:T(4,128)S(1)} all-gather(f32[16,4,4]{2,1,0:T(4,128)S(1)} %copy.87), channel_id=4, replica_groups=mesh['kv'=8,'tp'=4] {'kv'}, dimensions={0}, use_global_device_ids=true | all-gather | bytes 9216 | tf_op jit(solution)/shard_map/all_gather | solution.py:12
  124.1 31.0 %all-gather.1 = f32[128,4,4]{2,1,0:T(4,128)S(1)} all-gather(f32[16,4,4]{2,1,0:T(4,128)} %copy.86), channel_id=3, replica_groups=mesh['kv'=8,'tp'=4] {'kv'}, dimensions={0}, use_global_device_ids=true | all-gather | bytes 9216 | tf_op jit(solution)/shard_map/all_gather | solution.py:12
  155.4 1.9 reduce_window_sum.11
  157.3 26.2 %all-gather.5 = f32[8,16,4]{1,2,0:T(4,128)S(1)} all-gather(f32[1,16,4]{1,2,0:T(4,128)} %bitcast.112), channel_id=6, replica_groups=mesh['kv'=8,'tp'=4] {'kv'}, dimensions={0}, use_global_device_ids=true | all-gather | bytes 2304 | tf_op jit(solution)/shard_map/all_gather | solution.py:12
  183.5 1.0 multiply_convert_fusion.2
  184.6 1.0 fusion.41
  185.8 0.9 slice.23
  186.7 11.3 %while.21 = (s32[]{:T(128)}, f32[16,4,4]{0,2,1:T(4,128)S(1)}, f32[16,4,4]{0,2,1:T(4,128)S(1)}, f32[16,4,4,128]{3,2,1,0:T(4,128)S(1)}, f32[16,4]{0,1:T(4,128)S(1)...) while((s32[]{:T(128)}, f32[16,4,4]{0,2,1:T(4,128)S(1)}, ...), condition=%wide.region_7.8_spmd, body=%wide.region_6.7_spmd.sunk | while | flops 99909 | bytes 408483 | solution.py:18
  187.0 1.3 fusion.73
  188.6 1.3 fusion.73
  190.2 1.3 fusion.73
  191.8 1.3 fusion.73
  193.4 1.3 fusion.73
  195.1 1.3 fusion.73
  196.7 1.3 fusion.73
  199.0 1.9 convolution_convert_fusion.3
  201.0 28.8 %all-reduce.8.cloned.1.call-done = bf16[64,512]{1,0:T(8,128)(2,1)} async-done(((bf16[64,512]{1,0:T(8,128)(2,1)}), bf16[64,512]{1,0:T(8,128)(2,1)}) %all-reduce.8.cloned.1.call-update) | async-done | bytes 65552 | tf_op jit(solution)/shard_map/psum | solution.py:128
  229.8 1.0 fusion.32
  230.8 1.4 convolution_convert_fusion.1
  232.1 3.2 convolution_convert_fusion
  235.4 21.6 %psum.68 = bf16[64]{0:T(256)(128)(2,1)S(1)} all-reduce(bf16[64]{0:T(256)(128)(2,1)S(1)} %get-tuple-element.296), channel_id=1, replica_groups=mesh['kv'=8,'tp'=4] {'kv'}, use_global_device_ids=true, to_apply=%region_16.17 | all-reduce | flops 64 | bytes 256 | tf_op jit(solution)/shard_map/psum | solution.py:140
  257.0 53.1 %all-reduce.12.cloned.1.call-done = (bf16[64,2816]{1,0:T(8,128)(2,1)}, bf16[64,2816]{1,0:T(8,128)(2,1)}) async-done(((bf16[64,2816]{1,0:T(8,128)(2,1)}, bf16[64,2816]{1,0:T(8,128)(2,1)}), (bf16[64,2816]{1,0:T(8,128)(2,1)}, bf16[64,2816]{1,0:T(8,128)(2,1)})) %all-reduce.12.cloned.1.call-update) | async-done | bytes 720912 | tf_op jit(solution)/shard_map/psum | solution.py:139
  310.1 3.4 convolution_convert_fusion.2
  313.5 30.8 %all-reduce.10.cloned.1.call-done = bf16[64,512]{1,0:T(8,128)(2,1)} async-done(((bf16[64,512]{1,0:T(8,128)(2,1)}), bf16[64,512]{1,0:T(8,128)(2,1)}) %all-reduce.10.cloned.1.call-update) | async-done | bytes 65552 | tf_op jit(solution)/shard_map/psum | solution.py:145
  344.3 0.9 fusion.34
  345.1 0.7 reshape.117
  (80 shorter events, 6.8 us)
Async XLA Ops:
  6.5 224.2 %copy-start = (bf16[512,2816]{1,0:T(8,128)(2,1)S(1)}, bf16[512,2816]{1,0:T(8,128)(2,1)}, u32[]{:S(2)}) copy-start(bf16[512,2816]{1,0:T(8,128)(2,1)} %param.31) | copy-start | bytes 8650756
  6.5 177.0 %all-reduce.14.cloned.1.call-start = ((), (), s32[]{:S(2)}) async-start(), calls=%async_computation.4 | async-start | bytes 262144 | tf_op jit(solution)/shard_map/psum | solution.py:57
  12.0 173.8 %all-gather.8.cloned.1.call-start = ((), (), s32[]{:S(2)}) async-start(), calls=%async_computation.2 | async-start | bytes 1179648 | tf_op jit(solution)/shard_map/all_gather | solution.py:12
  39.7 0.6 copy-start.4
  74.6 8.5 %copy-start.5 = (bf16[16,512,512]{2,1,0:T(8,128)(2,1)S(1)}, bf16[16,512,512]{2,1,0:T(8,128)(2,1)}, u32[]{:S(2)}) copy-start(bf16[16,512,512]{2,1,0:T(8,128)(2,1)} %param.26) | copy-start | bytes 25165828
  76.3 8.1 %copy-start.2 = (bf16[16,4,4,128]{3,2,1,0:T(4,128)(2,1)}, bf16[16,4,4,128]{3,2,1,0:T(4,128)(2,1)S(1)}, u32[]{:S(2)}) copy-start(bf16[16,4,4,128]{3,2,1,0:T(4,128)(2,1)S(1)} %multiply_convert_fusion.4) | copy-start | bytes 196612
  82.5 0.6 copy-start.1
  85.1 144.7 %all-reduce.8.cloned.1.call-start = ((), (), s32[]{:S(2)}) async-start(), calls=%async_computation | async-start | bytes 131072 | tf_op jit(solution)/shard_map/psum | solution.py:128
  88.4 142.4 %copy-start.3 = (f32[512]{0:T(512)S(1)}, f32[512]{0:T(512)}, u32[]{:S(2)}) copy-start(f32[512]{0:T(512)} %param.30) | copy-start | bytes 6148
  200.9 109.1 %all-reduce.12.cloned.1.call-start = ((), (), s32[]{:S(2)}) async-start(), calls=%async_computation.3 | async-start | bytes 1441792 | tf_op jit(solution)/shard_map/psum | solution.py:139
  235.3 108.9 %all-reduce.10.cloned.1.call-start = ((), (), s32[]{:S(2)}) async-start(), calls=%async_computation.1 | async-start | bytes 131072 | tf_op jit(solution)/shard_map/psum | solution.py:145
Sparse Core Ops, SparseCore 0:
  12.1 73.4 all-reduce.13
  87.7 40.3 all-gather.7
  201.0 28.7 all-reduce.7
  235.5 74.5 all-reduce.11
  313.6 30.6 all-reduce.9
